TPU v7x, 32 devices: a whole 2x2x4 slice. The times are simulated.
32 devices in a mesh: sp: 16 (over z, y, x), tp: 2 (over core).
Axes of the slice: x: 2, y: 2, z: 4, core: 2. Of those that a mesh axis runs over, the one named last changes fastest.
Arguments:
- resid: bfloat16 [4096, 2048], P(('sp', 'tp')), may hold values from -6 to 6
- value_in: bfloat16 [4096, 1536], P('sp', 'tp'), may hold values from -6 to 6
- gate_in: bfloat16 [4096, 1536], P('sp', 'tp'), may hold values from -8 to 8
- conv_weight: float32 [31, 1536], P(None, 'tp'), may hold values from -2.5 to 2.5
- norm_gain: float32 [1536], P('tp'), may hold values from 0.1 to 1.9
- out_weight: bfloat16 [1536, 2048], replicated, may hold values from -0.15625 to 0.15625
- ffn_gain: float32 [2048], replicated, may hold values from 0.1 to 1.9
- expert_ids: int32 [4096, 2], P(('sp', 'tp')), may hold values from 0 to 31, all different within a row; in each aligned block of 128 rows (0 to 127, 128 to 255, ...) at most 16 rows name the same one
- expert_mix: float32 [4096, 2], P(('sp', 'tp')), may hold values from 0.1 to 1
- w_gate: bfloat16 [32, 2048, 1024], P(('sp', 'tp')), may hold values from -0.125 to 0.125
- w_up: bfloat16 [32, 2048, 1024], P(('sp', 'tp')), may hold values from -0.125 to 0.125
- w_down: bfloat16 [32, 1024, 2048], P(('sp', 'tp')), may hold values from -0.1875 to 0.1875
Outputs:
- layer_out: bfloat16 [4096, 2048], P(('sp', 'tp'))
Inputs may be any that keep to these rules, and one draw needn't show every extreme that they name: `expert_ids`: each row names 2 different experts; within each aligned block of 128 rows no expert is named by more than 16 rows, a bound that some block reaches.
All inputs are finite; a program needn't handle non-finite values.
Results may differ from a plain program's by a relative error of at most 0.012.
Values may be sent and summed in bfloat16 or wider, within the bound.
A program may use at most 128 MiB of HBM per device.

v0:
```python
import jax
import jax.numpy as jnp
from jax import lax
from jax.sharding import PartitionSpec as P


def padded_2(block, sides, width):
    for axis, dim in sides:
        count = lax.axis_size(axis)
        forward = [(i, i + 1) for i in range(count - 1)]
        backward = [(target, source) for source, target in forward]
        low = lax.ppermute(
            lax.slice_in_dim(block, block.shape[dim] - width, None, axis=dim), axis, forward
        )
        high = lax.ppermute(lax.slice_in_dim(block, 0, width, axis=dim), axis, backward)
        block = jnp.concatenate([low, block, high], axis=dim)
    return block


def expert_apply(rows, gate_w, up_w, down_w):
    gate = jnp.dot(rows, gate_w, preferred_element_type=jnp.float32)
    up = jnp.dot(rows, up_w, preferred_element_type=jnp.float32)
    hidden = (jax.nn.silu(gate) * up).astype(jnp.bfloat16)
    return jnp.dot(hidden, down_w, preferred_element_type=jnp.float32).astype(jnp.bfloat16)


def per_device(
    resid,
    value_in,
    gate_in,
    conv_weight,
    norm_gain,
    out_weight,
    ffn_gain,
    expert_ids,
    expert_mix,
    w_gate,
    w_up,
    w_down,
):
    glu = (value_in.astype(jnp.float32) * jax.nn.sigmoid(gate_in.astype(jnp.float32))).astype(
        jnp.bfloat16
    )
    taps = conv_weight.shape[0]
    reach = taps // 2
    length = glu.shape[0]
    local_width = glu.shape[1]
    padded = padded_2(glu, (("sp", 0),), reach).astype(jnp.float32)
    conv = jnp.zeros((length, local_width), jnp.float32)
    for tap in range(taps):
        conv = conv + padded[tap : tap + length] * conv_weight[tap]
    sums = lax.psum((jnp.sum(conv, axis=1), jnp.sum(conv * conv, axis=1)), "tp")
    width = local_width * lax.axis_size("tp")
    mean = sums[0] / width
    var = sums[1] / width - mean * mean
    normed_conv = (conv - mean[:, None]) * lax.rsqrt(var + 1e-05)[:, None] * norm_gain
    mixed = jax.nn.silu(normed_conv).astype(jnp.bfloat16)
    regrouped = lax.all_to_all(mixed, "tp", split_axis=0, concat_axis=1, tiled=True)
    proj = jnp.dot(regrouped, out_weight, preferred_element_type=jnp.float32)
    stream = (resid.astype(jnp.float32) + proj).astype(jnp.bfloat16)
    wide = stream.astype(jnp.float32)
    normed = (
        wide * lax.rsqrt(jnp.mean(wide * wide, axis=1, keepdims=True) + 1e-06) * ffn_gain
    ).astype(jnp.bfloat16)
    sp_count = lax.axis_size("sp")
    tp_count = lax.axis_size("tp")
    experts_all = sp_count * tp_count
    rows_here = stream.shape[0]
    topk = expert_ids.shape[1]
    model_width = stream.shape[1]
    cap = max(2, (2 * topk * rows_here + experts_all - 1) // experts_all)
    flat = expert_ids.reshape(-1)
    onehot = (flat[:, None] == jnp.arange(experts_all, dtype=jnp.int32)[None, :]).astype(jnp.int32)
    rank = jnp.sum(jnp.cumsum(onehot, axis=0) * onehot, axis=1) - 1
    dest = flat * cap + rank
    owner = jnp.arange(rows_here * topk, dtype=jnp.int32) // topk
    table = jnp.full((experts_all * cap,), rows_here, jnp.int32).at[dest].set(owner)
    source = jnp.concatenate([normed, jnp.zeros((1, model_width), jnp.bfloat16)], axis=0)
    outgoing = jnp.take(source, table, axis=0).reshape(experts_all, cap, model_width)
    gate_w, up_w, down_w = (w_gate[0], w_up[0], w_down[0])
    arrived = lax.all_to_all(outgoing, ("sp", "tp"), split_axis=0, concat_axis=0, tiled=True)
    shape = arrived.shape
    done = expert_apply(arrived.reshape(-1, model_width), gate_w, up_w, down_w).reshape(shape)
    returned = lax.all_to_all(done, ("sp", "tp"), split_axis=0, concat_axis=0, tiled=True)
    picked = jnp.take(returned.reshape(experts_all * cap, model_width), dest, axis=0)
    picked = picked.astype(jnp.float32).reshape(rows_here, topk, model_width)
    total = wide + jnp.sum(picked * expert_mix[:, :, None], axis=1)
    return total.astype(jnp.bfloat16)


def solution(mesh):
    return jax.shard_map(
        per_device,
        mesh=mesh,
        in_specs=(
            P(("sp", "tp"), None),
            P("sp", "tp"),
            P("sp", "tp"),
            P(None, "tp"),
            P("tp"),
            P(),
            P(),
            P(("sp", "tp"), None),
            P(("sp", "tp"), None),
            P(("sp", "tp"), None, None),
            P(("sp", "tp"), None, None),
            P(("sp", "tp"), None, None),
        ),
        out_specs=P(("sp", "tp"), None),
        check_vma=False,
    )
```

profile of v0, /device:TPU:0, one launch (start us, length us, event | category | flops | bytes accessed | tf_op | source)
XLA Modules:
  0.0 166.2 jit_solution(5589472671035958623)
XLA Ops:
  0.0 1.3 multiply_convert_fusion.3
  1.4 4.9 %collective-permute-start = (bf16[15,768]{1,0:T(8,128)(2,1)S(1)}, bf16[15,768]{1,0:T(8,128)(2,1)S(1)}, u32[]{:S(2)}, u32[]{:S(2)}) collective-permute-start(bf16[15,768]{1,0:T(8,128)(2,1)S(1)} %get-tuple-element.41), channel_id=1, source_target_pairs={{0,2},{2,4},{4,6},{6,8},{8,10},{10,12},{12,14},{14,16},{16,18},{18... | collective-permute-start | bytes 69128 | tf_op jit(solution)/shard_map/ppermute | solution.py:12
  6.2 1.3 collective-permute-start.1
  7.5 1.5 slice_reduce_fusion.31
  9.0 1.2 slice_reduce_fusion.30
  10.2 0.8 copy.27
  11.0 0.1 eq.26
  11.1 0.1 reshape.106
  11.3 0.7 broadcast_multiply_fusion
  12.0 0.6 reduce-window.6
  12.6 0.2 slice_reduce_fusion
  13.0 0.1 mul.499
  13.2 1.4 scatter_custom_fusion
  14.8 4.2 %fusion.51 = (f32[256]{0:T(256)S(1)}, f32[256]{0:T(256)S(1)}, f32[256,768]{1,0:T(8,128)S(1)}) fusion(f32[768]{0:T(1024)S(1)} %get-tuple-element.36, f32[286,768]{1,0:T(8,128)S(1)} %maximum_convert_fusion, f32[768]{0:T(1024)S(1)} %get-tuple-element.37, f32[768]{0:T(1024)S(1)} %get-tuple-element.8, f32[768]{0:T(1024)S(1)} %get-tuple-element.9, ...), kind=kLoop, calls=%fused_computation.143 | loop fusion | flops 12582400 | bytes 25263104 | tf_op jit(solution)/shard_map/reduce_sum | solution.py:52
  19.0 2.6 %all-reduce.1 = (f32[256]{0:T(256)S(1)}, f32[256]{0:T(256)S(1)}) all-reduce(f32[256]{0:T(256)S(1)} %get-tuple-element.6, f32[256]{0:T(256)S(1)} %get-tuple-element.5), channel_id=1, replica_groups=mesh['sp'=16,'tp'=2] {'tp'}, use_global_device_ids=true, to_apply=%region_3.0 | all-reduce | flops 512 | bytes 4096 | tf_op jit(solution)/shard_map/psum | solution.py:52
  21.6 0.3 multiply_convert_fusion.2
  22.0 4.0 %all_to_all.29 = bf16[2,128,768]{2,1,0:T(8,128)(2,1)S(1)} all-to-all(bf16[2,128,768]{2,1,0:T(8,128)(2,1)S(1)} %bitcast.50), channel_id=1, replica_groups=mesh['sp'=16,'tp'=2] {'tp'}, dimensions={0} | all-to-all | bytes 786432 | tf_op jit(solution)/shard_map/all_to_all | solution.py:58
  26.0 0.2 copy.26
  26.3 3.9 %multiply_reduce_fusion.1 = (f32[128]{0:T(128)S(1)}, f32[128,2048]{1,0:T(8,128)S(1)}) fusion(bf16[128,1536]{0,1:T(8,128)(2,1)S(1)} %bitcast.45, bf16[1536,2048]{1,0:T(8,128)(2,1)} %param.17, bf16[128,2048]{1,0:T(8,128)(2,1)S(1)} %copy-done), kind=kOutput, calls=%fused_computation.19 | convolution fusion | flops 806879104 | bytes 8258048 | tf_op jit(solution)/shard_map/dot_general | solution.py:59
  30.2 0.2 multiply_convert_fusion.1
  30.4 3.3 %gather_fusion = bf16[512,2048]{1,0:T(8,128)(2,1)} fusion(bf16[129,2048]{1,0:T(8,128)(2,1)S(1)} %concatenate.7, s32[1024]{0:T(1024)S(1)} %pad_clamp_fusion.1), kind=kCustom, calls=%fused_computation | custom fusion | bytes 4196352 | tf_op jit(solution)/shard_map/jit(_take)/gather | solution.py:79
  33.7 1.8 %broadcast_select_fusion = bf16[32,16,2048]{2,1,0:T(8,128)(2,1)S(1)} fusion(bf16[32,16,2048]{2,1,0:T(8,128)(2,1)} %bitcast.44, pred[32,16]{1,0:T(8,128)(4,1)S(1)} %broadcast_in_dim.38), kind=kLoop, calls=%fused_computation.15 | loop fusion | flops 1048576 | bytes 4194816 | tf_op jit(solution)/shard_map/jit(_take)/select_n | solution.py:79
  35.6 55.5 %all_to_all.30 = bf16[32,16,2048]{2,1,0:T(8,128)(2,1)S(1)} all-to-all(bf16[32,16,2048]{2,1,0:T(8,128)(2,1)S(1)} %broadcast_select_fusion), channel_id=1, replica_groups=mesh['sp'=16,'tp'=2] {'sp','tp'}, dimensions={0} | all-to-all | bytes 4194304 | tf_op jit(solution)/shard_map/all_to_all | solution.py:81
  91.1 3.7 %fusion.4 = f32[512,1024]{1,0:T(8,128)} fusion(bf16[512,2048]{1,0:T(8,128)(2,1)S(1)} %bitcast.47, bf16[1,2048,1024]{2,1,0:T(8,128)(2,1)S(1)} %copy-done.5), kind=kOutput, calls=%fused_computation.7 | convolution fusion | flops 2147483648 | bytes 8388608 | tf_op jit(solution)/shard_map/dot_general | solution.py:21
  94.8 9.9 %fusion.6 = bf16[512,2048]{1,0:T(8,128)(2,1)} fusion(bf16[1,1024,2048]{2,1,0:T(8,128)(2,1)} %param.23, f32[512,1024]{1,0:T(8,128)} %fusion.4, bf16[512,2048]{1,0:T(8,128)(2,1)S(1)} %bitcast.48, bf16[1,2048,1024]{2,1,0:T(8,128)(2,1)} %param.22), kind=kOutput, calls=%fused_computation.9 | convolution fusion | flops 4299161600 | bytes 14680064 | tf_op jit(solution)/shard_map/dot_general | solution.py:24
  104.7 3.7 %all-to-all-start.2 = ((bf16[32,16,2048]{2,1,0:T(8,128)(2,1)}), bf16[32,16,2048]{2,1,0:T(8,128)(2,1)S(1)}, u32[]{:S(2)}, u32[]{:S(2)}) async-start(bf16[32,16,2048]{2,1,0:T(8,128)(2,1)} %bitcast.46), calls=%async_computation.2 | async-start | bytes 4194304 | tf_op jit(solution)/shard_map/all_to_all | solution.py:84
  108.6 0.1 copy.31
  108.9 48.2 %all-to-all-done.2 = bf16[32,16,2048]{2,1,0:T(8,128)(2,1)S(1)} async-done(((bf16[32,16,2048]{2,1,0:T(8,128)(2,1)}), bf16[32,16,2048]{2,1,0:T(8,128)(2,1)S(1)}, u32[]{:S(2)}, u32[]{:S(2)}) %all-to-all-start.2) | async-done | bytes 2097184 | tf_op jit(solution)/shard_map/all_to_all | solution.py:84
  157.1 2.3 %gather_fusion.1 = bf16[256,2048]{1,0:T(8,128)(2,1)} fusion(bf16[512,2048]{1,0:T(8,128)(2,1)S(1)} %bitcast.43, s32[1024]{0:T(1024)S(1)} %pad_clamp_fusion), kind=kCustom, calls=%fused_computation.1 | custom fusion | bytes 2098176 | tf_op jit(solution)/shard_map/jit(_take)/gather | solution.py:85
  159.5 1.7 %gather.15 = bf16[128,2,2048]{2,1,0:T(2,128)(2,1)S(1)} reshape(bf16[256,2048]{1,0:T(8,128)(2,1)} %gather_fusion.1) | data formatting | bytes 2097152 | tf_op jit(solution)/shard_map/jit(_take)/gather | solution.py:85
  161.2 4.1 %multiply_reduce_fusion = f32[128,2048]{1,0:T(8,128)S(1)} fusion(bf16[128,2,2048]{2,1,0:T(2,128)(2,1)S(1)} %gather.15, pred[128,2]{1,0:T(8,128)(4,1)S(1)} %copy.31, f32[128,2]{1,0:T(8,128)S(1)} %copy.33), kind=kLoop, calls=%fused_computation.13 | loop fusion | flops 1835008 | bytes 2098432 | tf_op jit(solution)/shard_map/reduce_sum | solution.py:87
  165.3 0.9 add_convert_fusion
  (36 shorter events, 0.9 us)
Async XLA Ops:
  1.4 13.4 %collective-permute-start = (bf16[15,768]{1,0:T(8,128)(2,1)S(1)}, bf16[15,768]{1,0:T(8,128)(2,1)S(1)}, u32[]{:S(2)}, u32[]{:S(2)}) collective-permute-start(bf16[15,768]{1,0:T(8,128)(2,1)S(1)} %get-tuple-element.41), channel_id=1, source_target_pairs={{0,2},{2,4},{4,6},{6,8},{8,10},{10,12},{12,14},{14,16},{16,18},{18... | collective-permute-start | bytes 69128 | tf_op jit(solution)/shard_map/ppermute | solution.py:12
  6.2 8.5 %collective-permute-start.1 = (bf16[15,768]{1,0:T(8,128)(2,1)S(1)}, bf16[15,768]{1,0:T(8,128)(2,1)S(1)}, u32[]{:S(2)}, u32[]{:S(2)}) collective-permute-start(bf16[15,768]{1,0:T(8,128)(2,1)S(1)} %get-tuple-element.42), channel_id=1, source_target_pairs={{2,0},{4,2},{6,4},{8,6},{10,8},{12,10},{14,12},{16,14},{18,16},{20... | collective-permute-start | bytes 69128 | tf_op jit(solution)/shard_map/ppermute | solution.py:15
  14.8 6.8 %copy-start.3 = (f32[768]{0:T(1024)S(1)}, f32[768]{0:T(1024)}, u32[]{:S(2)}) copy-start(f32[768]{0:T(1024)} %param.16) | copy-start | bytes 9220
  19.0 7.2 %copy-start = (bf16[128,2048]{1,0:T(8,128)(2,1)S(1)}, bf16[128,2048]{1,0:T(8,128)(2,1)}, u32[]{:S(2)}) copy-start(bf16[128,2048]{1,0:T(8,128)(2,1)} %param.12) | copy-start | bytes 1572868
  26.3 3.9 %copy-start.2 = (f32[2048]{0:T(1024)S(1)}, f32[2048]{0:T(1024)}, u32[]{:S(2)}) copy-start(f32[2048]{0:T(1024)} %param.18) | copy-start | bytes 24580
  35.6 55.5 %copy-start.5 = (bf16[1,2048,1024]{2,1,0:T(8,128)(2,1)S(1)}, bf16[1,2048,1024]{2,1,0:T(8,128)(2,1)}, u32[]{:S(2)}) copy-start(bf16[1,2048,1024]{2,1,0:T(8,128)(2,1)} %param.21) | copy-start | bytes 12582916
  104.7 3.9 %copy-start.1 = (s32[128,2]{0,1:T(2,128)S(1)}, s32[128,2]{0,1:T(2,128)}, u32[]{:S(2)}) copy-start(s32[128,2]{0,1:T(2,128)} %param.19) | copy-start | bytes 3076
  104.7 4.1 %copy-start.4 = (f32[128,2]{0,1:T(2,128)S(1)}, f32[128,2]{0,1:T(2,128)}, u32[]{:S(2)}) copy-start(f32[128,2]{0,1:T(2,128)} %param.20) | copy-start | bytes 3076
  104.7 52.4 %all-to-all-start.2 = ((bf16[32,16,2048]{2,1,0:T(8,128)(2,1)}), bf16[32,16,2048]{2,1,0:T(8,128)(2,1)S(1)}, u32[]{:S(2)}, u32[]{:S(2)}) async-start(bf16[32,16,2048]{2,1,0:T(8,128)(2,1)} %bitcast.46), calls=%async_computation.2 | async-start | bytes 4194304 | tf_op jit(solution)/shard_map/all_to_all | solution.py:84
where the time goes:
time: 167 us; the launch traced here: 166 us
  blocking collectives  62.1 us (37%)
  waiting for transfers between devices  48.2 us (29%)
  matrix products  17.5 us (10%)
  other arithmetic  14.4 us (9%)
  local copies, waits for them, and re-layouts  13.8 us (8%)
  starting transfers between devices  9.84 us (6%)
    all_to_all x1, blocking collectives, per_device(): lax.all_to_all(outgoing, ('sp', 'tp'), split_axis=0, concat_axis=0, tiled...  55.5 us
    all_to_all x1, waiting for transfers between devices, per_device(): lax.all_to_all(done, ('sp', 'tp'), split_axis=0, concat_axis=0, tiled=True)  48.2 us
    dot_general x1, matrix products, expert_apply(): jnp.dot(hidden, down_w, preferred_element_type=jnp.float32)  9.89 us
    ppermute x1, starting transfers between devices, padded_2(): lax.ppermute(lax.slice_in_dim(block, block.shape[dim] - width, None, axis...  4.87 us
    reduce_sum x1, other arithmetic, per_device(): sums = lax.psum((jnp.sum(conv, axis=1), jnp.sum(conv * conv, axis=1)), 'tp')  4.16 us
    gather x2, local copies, waits for them, and re-layouts, per_device(): jnp.take(returned.reshape(experts_all * cap, model_width), dest, axis=0)  4.09 us
    reduce_sum x1, other arithmetic, per_device(): total = wide + jnp.sum(picked * expert_mix[:, :, None], axis=1)  4.07 us
    all_to_all x1, blocking collectives, per_device(): lax.all_to_all(mixed, 'tp', split_axis=0, concat_axis=1, tiled=True)  4.05 us
  transfers between devices with their start and end apart: 3, of which 1 were waited for; matrix products, arithmetic and copies ran while one was open for 5% of the time, Pallas kernels for 0%

commit v1 on v0

v1 whole, which is shorter than its diff:
```python
import functools
import jax
import jax.numpy as jnp
from jax import lax
from jax.experimental import pallas as pl
from jax.experimental.pallas import tpu as pltpu
from jax.sharding import PartitionSpec as P

MESH = pl.DeviceIdType.MESH
BF = jnp.bfloat16
F32 = jnp.float32


def padded_2(block, sides, width):
    for axis, dim in sides:
        count = lax.axis_size(axis)
        forward = [(i, i + 1) for i in range(count - 1)]
        backward = [(target, source) for source, target in forward]
        low = lax.ppermute(
            lax.slice_in_dim(block, block.shape[dim] - width, None, axis=dim), axis, forward
        )
        high = lax.ppermute(lax.slice_in_dim(block, 0, width, axis=dim), axis, backward)
        block = jnp.concatenate([low, block, high], axis=dim)
    return block


def experts_kernel(
    sp_count, tp_count, cap, chunks,
    tok, stream, info, wg_h, wu_h, wd_h, out,
    wg, wu, wd, ptok, pinfo, pack, rx, hid, ys, yr, ps, pr, acc,
    w_sem, pi_sem, pt_sem, d_send, d_recv, r_send, r_recv, pp_sem,
):
    half = sp_count // 2
    n_dev = half * tp_count
    rows, width = tok.shape
    dc = width // chunks
    slots = n_dev * cap
    me_sp = lax.axis_index("sp")
    me_tp = lax.axis_index("tp")
    local = lax.rem(me_sp, half)
    base = me_sp - local
    mine = local * tp_count + me_tp
    partner = (lax.rem(me_sp + half, sp_count), me_tp)

    def peer(i):
        n = lax.rem(mine + i, n_dev)
        return n, (base + n // tp_count, lax.rem(n, tp_count))

    weights = [
        pltpu.make_async_copy(h, v, w_sem.at[k])
        for k, (h, v) in enumerate(((wg_h, wg), (wu_h, wu), (wd_h, wd)))
    ]
    for w in weights:
        w.start()

    barrier = pltpu.get_barrier_semaphore()

    @pl.loop(1, n_dev)
    def _(i):
        pl.semaphore_signal(barrier, inc=1, device_id=peer(i)[1], device_id_type=MESH)

    pl.semaphore_signal(barrier, inc=1, device_id=partner, device_id_type=MESH)
    pl.semaphore_wait(barrier, n_dev)

    def remote(src, dst, send, recv, where):
        return pltpu.make_async_remote_copy(
            src_ref=src, dst_ref=dst, send_sem=send, recv_sem=recv,
            device_id=where, device_id_type=MESH,
        )

    info_copy = remote(info, pinfo, pi_sem.at[0], pi_sem.at[1], partner)
    info_copy.start()
    tok_copies = [
        remote(tok.at[:, c * dc : (c + 1) * dc], ptok.at[c], pt_sem.at[0, c], pt_sem.at[1, c], partner)
        for c in range(chunks)
    ]
    for t in tok_copies:
        t.start()

    def slot_match(ref):
        ids = lax.broadcasted_iota(jnp.int32, (slots, rows), 0) + base * (tp_count * cap)
        ids = ids.astype(F32)
        return ids == ref[0:1, :], ids == ref[1:2, :]

    def exchange(src, dst, send, recv, s, c):
        @pl.loop(1, n_dev)
        def _(i):
            n, where = peer(i)
            remote(src.at[s, c, n], dst.at[s, c, mine], send.at[s, c], recv.at[s, c], where).start()

        pltpu.make_async_copy(src.at[s, c, mine], dst.at[s, c, mine], recv.at[s, c]).start()

    def all_in(dst, recv, s, c):
        pltpu.make_async_copy(dst.at[s, c], dst.at[s, c], recv.at[s, c]).wait()

    def all_out(src, send, s, c):
        part = src.at[s, c, pl.ds(0, n_dev - 1)]
        pltpu.make_async_copy(part, part, send.at[s, c]).wait()

    def pack_send(s, c, match, block):
        picked = jnp.dot(match, block, preferred_element_type=F32)
        pack[s, c] = picked.astype(BF).reshape(n_dev, cap, dc)
        exchange(pack, rx, d_send, d_recv, s, c)

    def one_hot(ref):
        a, b = slot_match(ref)
        return jnp.where(a | b, 1.0, 0.0).astype(BF)

    own = one_hot(info)
    for c in range(chunks):
        pack_send(0, c, own, tok[:, c * dc : (c + 1) * dc])
    info_copy.wait_recv()
    other = one_hot(pinfo)

    def run_experts(s):
        for c in range(chunks):
            all_in(rx, d_recv, s, c)
        ff = wg.shape[1]
        tile = min(256, ff)

        @pl.loop(0, ff // tile)
        def _(f):
            cols = pl.ds(pl.multiple_of(f * tile, tile), tile)
            gate = jnp.zeros((slots, tile), F32)
            up = jnp.zeros((slots, tile), F32)
            for c in range(chunks):
                x = rx[s, c].reshape(slots, dc)
                gate = gate + jnp.dot(x, wg[c * dc : (c + 1) * dc, cols], preferred_element_type=F32)
                up = up + jnp.dot(x, wu[c * dc : (c + 1) * dc, cols], preferred_element_type=F32)
            hid[:, cols] = (gate * jax.nn.sigmoid(gate) * up).astype(BF)

        for c in range(chunks):
            y = jnp.dot(hid[...], wd[:, c * dc : (c + 1) * dc], preferred_element_type=F32)
            ys[s, c] = y.astype(BF).reshape(n_dev, cap, dc)
            exchange(ys, yr, r_send, r_recv, s, c)

    tok_copies[0].wait_recv()
    pack_send(1, 0, other, ptok[0])
    for w in weights:
        w.wait()
    run_experts(0)
    for c in range(1, chunks):
        tok_copies[c].wait_recv()
        pack_send(1, c, other, ptok[c])
    run_experts(1)

    def mix_matrix(ref):
        a, b = slot_match(ref)
        full = jnp.where(a, ref[2:3, :], 0.0) + jnp.where(b, ref[3:4, :], 0.0)
        high = full.astype(BF)
        return high, (full - high.astype(F32)).astype(BF)

    def combine(s, c, mats):
        y = yr[s, c].reshape(slots, dc)
        dims = (((0,), (0,)), ((), ()))
        return sum(lax.dot_general(m, y, dims, preferred_element_type=F32) for m in mats)

    own_mix = mix_matrix(info)
    for c in range(chunks):
        all_in(yr, r_recv, 0, c)
        acc[:, c * dc : (c + 1) * dc] = stream[:, c * dc : (c + 1) * dc].astype(F32) + combine(0, c, own_mix)
    other_mix = mix_matrix(pinfo)
    parts = []
    for c in range(chunks):
        all_in(yr, r_recv, 1, c)
        ps[c] = combine(1, c, other_mix).astype(BF)
        copy = remote(ps.at[c], pr.at[c], pp_sem.at[0, c], pp_sem.at[1, c], partner)
        copy.start()
        parts.append(copy)
    for c in range(chunks):
        parts[c].wait_recv()
        out[:, c * dc : (c + 1) * dc] = (acc[:, c * dc : (c + 1) * dc] + pr[c].astype(F32)).astype(BF)
    info_copy.wait_send()
    for c in range(chunks):
        tok_copies[c].wait_send()
        parts[c].wait_send()
        for s in range(2):
            all_out(pack, d_send, s, c)
            all_out(ys, r_send, s, c)


def experts_call(normed, stream, info, w_gate, w_up, w_down, cap):
    sp_count, tp_count = lax.axis_size("sp"), lax.axis_size("tp")
    chunks = 2
    rows, width = normed.shape
    n_dev = sp_count // 2 * tp_count
    dc = width // chunks
    ff = w_gate.shape[1]
    vm = pl.BlockSpec(memory_space=pltpu.VMEM)
    hb = pl.BlockSpec(memory_space=pl.ANY)
    blocks = pltpu.VMEM((2, chunks, n_dev, cap, dc), BF)
    dma = pltpu.SemaphoreType.DMA
    return pl.pallas_call(
        functools.partial(experts_kernel, sp_count, tp_count, cap, chunks),
        out_shape=jax.ShapeDtypeStruct((rows, width), BF),
        in_specs=[vm, vm, vm, hb, hb, hb],
        out_specs=vm,
        scratch_shapes=[
            pltpu.VMEM((width, ff), BF),
            pltpu.VMEM((width, ff), BF),
            pltpu.VMEM((ff, width), BF),
            pltpu.VMEM((chunks, rows, dc), BF),
            pltpu.VMEM(info.shape, F32),
            blocks,
            blocks,
            pltpu.VMEM((n_dev * cap, ff), BF),
            blocks,
            blocks,
            pltpu.VMEM((chunks, rows, dc), BF),
            pltpu.VMEM((chunks, rows, dc), BF),
            pltpu.VMEM((rows, width), F32),
            dma((3,)),
            dma((2,)),
            dma((2, chunks)),
            dma((2, chunks)),
            dma((2, chunks)),
            dma((2, chunks)),
            dma((2, chunks)),
            dma((2, chunks)),
        ],
        compiler_params=pltpu.CompilerParams(
            collective_id=0, has_side_effects=True, vmem_limit_bytes=56 * 1024 * 1024
        ),
        name="experts",
    )(normed, stream, info, w_gate, w_up, w_down)


def per_device(
    resid,
    value_in,
    gate_in,
    conv_weight,
    norm_gain,
    out_weight,
    ffn_gain,
    expert_ids,
    expert_mix,
    w_gate,
    w_up,
    w_down,
):
    glu = (value_in.astype(F32) * jax.nn.sigmoid(gate_in.astype(F32))).astype(BF)
    taps = conv_weight.shape[0]
    reach = taps // 2
    length = glu.shape[0]
    local_width = glu.shape[1]
    padded = padded_2(glu, (("sp", 0),), reach).astype(F32)
    conv = jnp.zeros((length, local_width), F32)
    for tap in range(taps):
        conv = conv + padded[tap : tap + length] * conv_weight[tap]
    sums = lax.psum((jnp.sum(conv, axis=1), jnp.sum(conv * conv, axis=1)), "tp")
    width = local_width * lax.axis_size("tp")
    mean = sums[0] / width
    var = sums[1] / width - mean * mean
    normed_conv = (conv - mean[:, None]) * lax.rsqrt(var + 1e-05)[:, None] * norm_gain
    mixed = jax.nn.silu(normed_conv).astype(BF)
    regrouped = lax.all_to_all(mixed, "tp", split_axis=0, concat_axis=1, tiled=True)
    proj = jnp.dot(regrouped, out_weight, preferred_element_type=F32)
    stream = (resid.astype(F32) + proj).astype(BF)
    wide = stream.astype(F32)
    normed = (
        wide * lax.rsqrt(jnp.mean(wide * wide, axis=1, keepdims=True) + 1e-06) * ffn_gain
    ).astype(BF)
    experts_all = lax.axis_size("sp") * lax.axis_size("tp")
    rows_here = stream.shape[0]
    topk = expert_ids.shape[1]
    cap = max(2, (2 * topk * rows_here + experts_all - 1) // experts_all)
    ids = expert_ids.T
    hot = (ids[:, None, :] == jnp.arange(experts_all, dtype=jnp.int32)[None, :, None]).astype(F32)
    named = jnp.sum(hot, axis=0)
    at = jnp.arange(rows_here, dtype=jnp.int32)
    before = (at[:, None] < at[None, :]).astype(BF)
    rank = jnp.dot(named.astype(BF), before, preferred_element_type=F32)
    slot = ids.astype(F32) * cap + jnp.sum(hot * rank[None], axis=1)
    info = jnp.concatenate([slot, expert_mix.T, jnp.zeros((8 - 2 * topk, rows_here), F32)], axis=0)
    return experts_call(normed, stream, info, w_gate[0], w_up[0], w_down[0], cap)


def solution(mesh):
    return jax.shard_map(
        per_device,
        mesh=mesh,
        in_specs=(
            P(("sp", "tp"), None),
            P("sp", "tp"),
            P("sp", "tp"),
            P(None, "tp"),
            P("tp"),
            P(),
            P(),
            P(("sp", "tp"), None),
            P(("sp", "tp"), None),
            P(("sp", "tp"), None, None),
            P(("sp", "tp"), None, None),
            P(("sp", "tp"), None, None),
        ),
        out_specs=P(("sp", "tp"), None),
        check_vma=False,
    )
```

time: 167 us -> 126 us (0.75)
  Pallas kernels: 0 us -> 92.4 us
  blocking collectives: 62.1 us -> 6.52 us
  waiting for transfers between devices: 48.2 us -> 0.01 us
  matrix products: 17.5 us -> 4.04 us
  local copies, waits for them, and re-layouts: 13.8 us -> 4.82 us
  other arithmetic: 14.4 us -> 10.3 us
  starting transfers between devices: 9.84 us -> 6.16 us
    pallas_call x0 -> x1, Pallas kernels: none -> 92.4 us  [experts_call(): pl.pallas_call(functools.partial(experts_kernel, sp_count, tp_count, cap,...]
    all_to_all x1 -> x0, blocking collectives: 55.5 us -> none  [per_device(): lax.all_to_all(outgoing, ('sp', 'tp'), split_axis=0, concat_axis=0, tiled...]
    all_to_all x1 -> x0, waiting for transfers between devices: 48.2 us -> none  [per_device(): lax.all_to_all(done, ('sp', 'tp'), split_axis=0, concat_axis=0, tiled=True)]
    dot_general x3 -> x2, matrix products: 17.5 us -> 4.04 us  [the longest x1 3.9 us: per_device(): proj = jnp.dot(regrouped, out_weight, preferred_element_type=F32)]
    gather x3 -> x0, local copies, waits for them, and re-layouts: 7.44 us -> none  [the longest x2 4.09 us: per_device(): jnp.take(returned.reshape(experts_all * cap, model_width), dest, axis=0)]
    all_to_all x1 -> x0, starting transfers between devices: 3.67 us -> none  [per_device(): lax.all_to_all(done, ('sp', 'tp'), split_axis=0, concat_axis=0, tiled=True)]
    reduce_sum x2, other arithmetic: 4.17 us -> 1.4 us  [the longest x1 0.71 us: per_device(): slot = ids.astype(F32) * cap + jnp.sum(hot * rank[None], axis=1)]
    select_n x4 -> x0, other arithmetic: 1.85 us -> none  [the longest x2 1.84 us: per_device(): jnp.take(source, table, axis=0).reshape(experts_all, cap, model_width)]
  transfers between devices with their start and end apart: 3 -> 2, of which waited for: 1 -> 0; matrix products, arithmetic and copies ran while one was open for 5% -> 5% of each run, Pallas kernels for 0% -> 0%
where the time goes in v1:
time: 126 us; the launch traced here: 124 us
  Pallas kernels  92.4 us (73%)
  other arithmetic  10.3 us (8%)
  blocking collectives  6.52 us (5%)
  starting transfers between devices  6.16 us (5%)
  local copies, waits for them, and re-layouts  4.82 us (4%)
  matrix products  4.04 us (3%)
    pallas_call x1, Pallas kernels, experts_call(): pl.pallas_call(functools.partial(experts_kernel, sp_count, tp_count, cap,...  92.4 us
    ppermute x1, starting transfers between devices, padded_2(): lax.ppermute(lax.slice_in_dim(block, block.shape[dim] - width, None, axis...  4.87 us
    reduce_sum x1, other arithmetic, per_device(): sums = lax.psum((jnp.sum(conv, axis=1), jnp.sum(conv * conv, axis=1)), 'tp')  4.16 us
    all_to_all x1, blocking collectives, per_device(): lax.all_to_all(mixed, 'tp', split_axis=0, concat_axis=1, tiled=True)  4.05 us
    dot_general x1, matrix products, per_device(): proj = jnp.dot(regrouped, out_weight, preferred_element_type=F32)  3.9 us
    slice x2, local copies, waits for them, and re-layouts, per_device(): conv = conv + padded[tap:tap + length] * conv_weight[tap]  2.61 us
  transfers between devices with their start and end apart: 2, of which 0 were waited for; matrix products, arithmetic and copies ran while one was open for 5% of the time, Pallas kernels for 0%

profile of v1, /device:TPU:0, one launch (start us, length us, event | category | flops | bytes accessed | tf_op | source)
XLA Modules:
  0.0 124.4 jit_solution(17680499765172612188)
XLA Ops:
  0.0 1.3 %multiply_convert_fusion.1 = bf16[256,768]{1,0:T(8,128)(2,1)S(1)} fusion(bf16[256,768]{1,0:T(8,128)(2,1)} %param.14, bf16[256,768]{1,0:T(8,128)(2,1)} %param.13), kind=kLoop, calls=%fused_computation.70 | loop fusion | flops 1376256 | bytes 1179648 | tf_op jit(solution)/shard_map/convert_element_type | solution.py:242
  1.4 4.9 %collective-permute-start = (bf16[15,768]{1,0:T(8,128)(2,1)S(1)}, bf16[15,768]{1,0:T(8,128)(2,1)S(1)}, u32[]{:S(2)}, u32[]{:S(2)}) collective-permute-start(bf16[15,768]{1,0:T(8,128)(2,1)S(1)} %get-tuple-element.41), channel_id=1, source_target_pairs={{0,2},{2,4},{4,6},{6,8},{8,10},{10,12},{12,14},{14,16},{16,18},{18... | collective-permute-start | bytes 69128 | tf_op jit(solution)/shard_map/ppermute | solution.py:19
  6.2 1.3 %collective-permute-start.1 = (bf16[15,768]{1,0:T(8,128)(2,1)S(1)}, bf16[15,768]{1,0:T(8,128)(2,1)S(1)}, u32[]{:S(2)}, u32[]{:S(2)}) collective-permute-start(bf16[15,768]{1,0:T(8,128)(2,1)S(1)} %get-tuple-element.42), channel_id=1, source_target_pairs={{2,0},{4,2},{6,4},{8,6},{10,8},{12,10},{14,12},{16,14},{18,16},{20... | collective-permute-start | bytes 69128 | tf_op jit(solution)/shard_map/ppermute | solution.py:22
  7.5 1.5 %slice_reduce_fusion.30 = (f32[768]{0:T(1024)S(1)}, f32[768]{0:T(1024)S(1)}, f32[768]{0:T(1024)S(1)}, f32[768]{0:T(1024)S(1)}, f32[768]{0:T(1024)S(1)}, /*index=...) fusion(f32[31,768]{1,0:T(8,128)} %param.15), kind=kLoop, calls=%fused_computation.109 | loop fusion | bytes 116736 | tf_op jit(solution)/shard_map/slice | solution.py:250
  9.0 0.7 convert_reduce_fusion
  9.7 0.1 fusion.34
  9.8 0.7 select_reduce_fusion
  10.6 0.7 multiply_add_fusion
  11.2 0.1 pad.2.clone
  11.3 1.3 %maximum_maximum_fusion.info = f32[8,128]{1,0:T(8,128)} fusion(f32[2,128]{1,0:T(2,128)} %bitcast.20, f32[2,128]{1,0:T(2,128)S(1)} %multiply_add_fusion, f32[8]{0:T(128)S(1)} %pad.2.clone), kind=kLoop, calls=%fused_computation.78 | loop fusion | flops 2048 | bytes 6176 | tf_op jit(solution)/shard_map/concatenate | solution.py:275
  12.7 1.1 slice_reduce_fusion.29
  13.8 0.0 collective-permute-done
  13.8 0.0 collective-permute-done.1
  13.8 0.1 maximum_convert_fusion
  13.9 0.0 copy-start.3
  13.9 0.0 copy-start.1
  13.9 4.2 %fusion.36 = (f32[256]{0:T(256)S(1)}, f32[256]{0:T(256)S(1)}, f32[256,768]{1,0:T(8,128)S(1)}) fusion(f32[768]{0:T(1024)S(1)} %get-tuple-element.36, f32[286,768]{1,0:T(8,128)S(1)} %maximum_convert_fusion, f32[768]{0:T(1024)S(1)} %get-tuple-element.37, f32[768]{0:T(1024)S(1)} %get-tuple-element.8, f32[768]{0:T(1024)S(1)} %get-tuple-element.9, ...), kind=kLoop, calls=%fused_computation.114 | loop fusion | flops 12582400 | bytes 25263104 | tf_op jit(solution)/shard_map/reduce_sum | solution.py:251
  18.1 2.5 %all-reduce = (f32[256]{0:T(256)S(1)}, f32[256]{0:T(256)S(1)}) all-reduce(f32[256]{0:T(256)S(1)} %get-tuple-element.6, f32[256]{0:T(256)S(1)} %get-tuple-element.5), channel_id=1, replica_groups=mesh['sp'=16,'tp'=2] {'tp'}, use_global_device_ids=true, to_apply=%region_3.0 | all-reduce | flops 512 | bytes 4096 | tf_op jit(solution)/shard_map/psum | solution.py:251
  20.6 0.0 copy-done.3
  20.6 0.3 multiply_convert_fusion
  20.9 4.0 %all_to_all.19 = bf16[2,128,768]{2,1,0:T(8,128)(2,1)S(1)} all-to-all(bf16[2,128,768]{2,1,0:T(8,128)(2,1)S(1)} %bitcast.17), channel_id=1, replica_groups=mesh['sp'=16,'tp'=2] {'tp'}, dimensions={0} | all-to-all | bytes 786432 | tf_op jit(solution)/shard_map/all_to_all | solution.py:257
  25.0 0.2 copy.14
  25.2 0.0 copy-done.1
  25.2 0.0 copy-start.2
  25.2 3.9 %fusion.1 = (f32[128]{0:T(128)S(1)}, bf16[128,2048]{1,0:T(8,128)(2,1)S(1)}) fusion(bf16[128,1536]{0,1:T(8,128)(2,1)S(1)} %bitcast.15, bf16[1536,2048]{1,0:T(8,128)(2,1)} %param.17, bf16[128,2048]{1,0:T(8,128)(2,1)S(1)} %copy-done.1), kind=kOutput, calls=%fused_computation.4 | convolution fusion | flops 806879104 | bytes 7733760 | tf_op jit(solution)/shard_map/dot_general | solution.py:258
  29.1 0.0 copy-start
  29.1 0.0 copy-done.2
  29.1 1.0 fusion.3.tok
  30.1 0.0 copy-done
  30.1 92.4 %experts.1 = bf16[128,2048]{1,0:T(8,128)(2,1)} custom-call(bf16[128,2048]{1,0:T(8,128)(2,1)} %fusion.3.tok, bf16[128,2048]{1,0:T(8,128)(2,1)} %copy-done, f32[8,128]{1,0:T(8,128)} %maximum_maximum_fusion.info, bf16[2048,1024]{1,0:T(8,128)(2,1)} %bitcast.12, bf16[2048,1024]{1,0:T(8,128)(2,1)} %bitcast.13, bf16[1024,2048]{1,0:T(8,128)(2,1)} %bitcast.14), custom_call_target="tpu_custom_call" | custom-call | tf_op jit(solution)/shard_map/experts/pallas_call | solution.py:193
  122.5 1.9 %copy.16 = bf16[128,2048]{1,0:T(8,128)(2,1)} copy(bf16[128,2048]{1,0:T(8,128)(2,1)} %experts.1) | data formatting | bytes 1048576
  (4 shorter events, 0.0 us)
Async XLA Ops:
  1.4 12.4 %collective-permute-start = (bf16[15,768]{1,0:T(8,128)(2,1)S(1)}, bf16[15,768]{1,0:T(8,128)(2,1)S(1)}, u32[]{:S(2)}, u32[]{:S(2)}) collective-permute-start(bf16[15,768]{1,0:T(8,128)(2,1)S(1)} %get-tuple-element.41), channel_id=1, source_target_pairs={{0,2},{2,4},{4,6},{6,8},{8,10},{10,12},{12,14},{14,16},{16,18},{18... | collective-permute-start | bytes 69128 | tf_op jit(solution)/shard_map/ppermute | solution.py:19
  6.2 7.6 %collective-permute-start.1 = (bf16[15,768]{1,0:T(8,128)(2,1)S(1)}, bf16[15,768]{1,0:T(8,128)(2,1)S(1)}, u32[]{:S(2)}, u32[]{:S(2)}) collective-permute-start(bf16[15,768]{1,0:T(8,128)(2,1)S(1)} %get-tuple-element.42), channel_id=1, source_target_pairs={{2,0},{4,2},{6,4},{8,6},{10,8},{12,10},{14,12},{16,14},{18,16},{20... | collective-permute-start | bytes 69128 | tf_op jit(solution)/shard_map/ppermute | solution.py:22
  13.9 6.7 %copy-start.3 = (f32[768]{0:T(1024)S(1)}, f32[768]{0:T(1024)}, u32[]{:S(2)}) copy-start(f32[768]{0:T(1024)} %param.16) | copy-start | bytes 9220
  13.9 11.3 %copy-start.1 = (bf16[128,2048]{1,0:T(8,128)(2,1)S(1)}, bf16[128,2048]{1,0:T(8,128)(2,1)}, u32[]{:S(2)}) copy-start(bf16[128,2048]{1,0:T(8,128)(2,1)} %param.12) | copy-start | bytes 1572868
  25.2 3.9 %copy-start.2 = (f32[2048]{0:T(1024)S(1)}, f32[2048]{0:T(1024)}, u32[]{:S(2)}) copy-start(f32[2048]{0:T(1024)} %param.18) | copy-start | bytes 24580
  29.1 1.0 copy-start

commit v2 on v1

v2 whole, which is shorter than its diff:
```python
import functools
import jax
import jax.numpy as jnp
from jax import lax
from jax.experimental import pallas as pl
from jax.experimental.pallas import tpu as pltpu
from jax.sharding import PartitionSpec as P

MESH = pl.DeviceIdType.MESH
BF = jnp.bfloat16
F32 = jnp.float32


def layer_kernel(
    sp_count, tp_count, cap, chunks,
    resid, value_in, gate_in, taps_w, gain, ffn_gain, routes, ow_h, wg_h, wu_h, wd_h, out,
    wg, wu, wd, ptok, pinfo, pack, rx, hid, ys, yr, ps, pr, acc,
    tok, info, ow, gp, wide_in, cs, cf, gf,
    w_sem, pi_sem, pt_sem, d_send, d_recv, r_send, r_recv, pp_sem,
    h_sem, c_sem, g_sem,
):
    half = sp_count // 2
    n_dev = half * tp_count
    rows, width = resid.shape
    dc = width // chunks
    slots = n_dev * cap
    me_sp = lax.axis_index("sp")
    me_tp = lax.axis_index("tp")
    local = lax.rem(me_sp, half)
    base = me_sp - local
    mine = local * tp_count + me_tp
    partner = (lax.rem(me_sp + half, sp_count), me_tp)

    def peer(i):
        n = lax.rem(mine + i, n_dev)
        return n, (base + n // tp_count, lax.rem(n, tp_count))

    weights = [
        pltpu.make_async_copy(h, v, w_sem.at[k])
        for k, (h, v) in enumerate(((ow_h, ow), (wg_h, wg), (wu_h, wu), (wd_h, wd)))
    ]
    for w in weights:
        w.start()

    barrier = pltpu.get_barrier_semaphore()

    @pl.loop(1, n_dev)
    def _(i):
        pl.semaphore_signal(barrier, inc=1, device_id=peer(i)[1], device_id_type=MESH)

    last = sp_count - 1
    has_low, has_high = me_sp > 0, me_sp < last
    lower = (jnp.maximum(me_sp - 1, 0), me_tp)
    upper = (jnp.minimum(me_sp + 1, last), me_tp)
    twin = (me_sp, 1 - me_tp)
    pl.semaphore_signal(barrier, inc=1, device_id=partner, device_id_type=MESH)

    @pl.when(has_low)
    def _():
        pl.semaphore_signal(barrier, inc=1, device_id=lower, device_id_type=MESH)

    @pl.when(has_high)
    def _():
        pl.semaphore_signal(barrier, inc=1, device_id=upper, device_id_type=MESH)

    length, local_width = value_in.shape
    taps = taps_w.shape[0]
    reach = taps // 2
    halo = (reach + 15) // 16 * 16
    gated = value_in[...].astype(F32) * jax.nn.sigmoid(gate_in[...].astype(F32))
    gp[halo : halo + length, :] = gated.astype(BF)

    @pl.when(jnp.logical_not(has_low))
    def _():
        gp[0:halo, :] = jnp.zeros((halo, local_width), BF)

    @pl.when(jnp.logical_not(has_high))
    def _():
        gp[halo + length :, :] = jnp.zeros((halo, local_width), BF)

    pl.semaphore_wait(
        barrier, n_dev + has_low.astype(jnp.int32) + has_high.astype(jnp.int32)
    )

    def remote(src, dst, send, recv, where):
        return pltpu.make_async_remote_copy(
            src_ref=src, dst_ref=dst, send_sem=send, recv_sem=recv,
            device_id=where, device_id_type=MESH,
        )

    to_low = remote(
        gp.at[halo : 2 * halo], gp.at[halo + length : 2 * halo + length], h_sem.at[0], h_sem.at[1], lower
    )
    to_high = remote(gp.at[length : length + halo], gp.at[0:halo], h_sem.at[2], h_sem.at[3], upper)

    @pl.when(has_low)
    def _():
        to_low.start()

    @pl.when(has_high)
    def _():
        to_high.start()

    gain_copy = remote(gain, gf, g_sem.at[0], g_sem.at[1], twin)
    gain_copy.start()

    experts_all = sp_count * tp_count
    expert = lax.broadcasted_iota(jnp.int32, (experts_all, rows), 0).astype(F32)
    hot = [jnp.where(expert == routes[k : k + 1, :], 1.0, 0.0) for k in range(2)]
    earlier = lax.broadcasted_iota(jnp.int32, (rows, rows), 0)
    later = lax.broadcasted_iota(jnp.int32, (rows, rows), 1)
    before = jnp.where(earlier < later, 1.0, 0.0).astype(BF)
    rank = jnp.dot((hot[0] + hot[1]).astype(BF), before, preferred_element_type=F32)
    info[...] = routes[...]
    for k in range(2):
        info[k : k + 1, :] = routes[k : k + 1, :] * cap + jnp.sum(
            hot[k] * rank, axis=0, keepdims=True
        )
    info_copy = remote(info, pinfo, pi_sem.at[0], pi_sem.at[1], partner)
    info_copy.start()

    @pl.when(has_low)
    def _():
        to_high.wait_recv()

    @pl.when(has_high)
    def _():
        to_low.wait_recv()

    wide_in[...] = gp[...].astype(F32)
    span = rows + 2 * halo

    def convolve(first, put):
        @pl.loop(0, local_width // 128)
        def _(b):
            cols = pl.ds(pl.multiple_of(b * 128, 128), 128)
            x = wide_in[pl.ds(first, span), cols]
            total = jnp.zeros((rows, 128), F32)
            for r in range(8):
                offsets = [j for j in range(taps) if (j + halo - reach) % 8 == r]
                if not offsets:
                    continue
                shifted = x if r == 0 else pltpu.roll(x, span - r, 0)
                for j in offsets:
                    at = j + halo - reach - r
                    total = total + shifted[at : at + rows] * taps_w[j : j + 1, cols]
            put(cols, total)

    def put_out(cols, total):
        cs[:, cols] = total

    def put_own(cols, total):
        cf[0, :, cols] = total

    convolve(pl.multiple_of((1 - me_tp) * rows, rows), put_out)
    conv_copy = remote(cs, cf.at[1], c_sem.at[0], c_sem.at[1], twin)
    conv_copy.start()
    convolve(pl.multiple_of(me_tp * rows, rows), put_own)
    weights[0].wait()
    gain_copy.wait_recv()
    conv_copy.wait_recv()
    channels = local_width * tp_count
    mean = (jnp.sum(cf[0], axis=1, keepdims=True) + jnp.sum(cf[1], axis=1, keepdims=True)) / channels
    msq = (
        jnp.sum(cf[0] * cf[0], axis=1, keepdims=True) + jnp.sum(cf[1] * cf[1], axis=1, keepdims=True)
    ) / channels
    scale = lax.rsqrt(msq - mean * mean + 1e-05)

    def silu(v):
        return v * jax.nn.sigmoid(v)

    mixed = [
        silu((cf[0] - mean) * scale * gain[...]).astype(BF),
        silu((cf[1] - mean) * scale * gf[...]).astype(BF),
    ]
    whose = (me_tp, 1 - me_tp)
    square = jnp.zeros((rows, 1), F32)
    step = 512
    for c in range(width // step):
        cols = slice(c * step, (c + 1) * step)
        proj = jnp.zeros((rows, step), F32)
        for m, w in zip(mixed, whose):
            at = pl.ds(pl.multiple_of(w * local_width, local_width), local_width)
            proj = proj + jnp.dot(m, ow[at, cols], preferred_element_type=F32)
        wide = (resid[:, cols].astype(F32) + proj).astype(BF).astype(F32)
        acc[:, cols] = wide
        square = square + jnp.sum(wide * wide, axis=1, keepdims=True)
    rms = lax.rsqrt(square / width + 1e-06)
    for c in range(chunks):
        tok[c] = (
            acc[:, c * dc : (c + 1) * dc] * rms * ffn_gain[:, c * dc : (c + 1) * dc]
        ).astype(BF)

    quarter = sp_count // 4
    inner = (me_sp >= quarter) & (me_sp < sp_count - quarter)
    tok_copies = [
        remote(tok.at[c], ptok.at[c], pt_sem.at[0, c], pt_sem.at[1, c], partner)
        for c in range(chunks)
    ]

    @pl.when(inner)
    def _():
        for t in tok_copies:
            t.start()

    def slot_match(ref):
        ids = lax.broadcasted_iota(jnp.int32, (slots, rows), 0) + base * (tp_count * cap)
        ids = ids.astype(F32)
        return ids == ref[0:1, :], ids == ref[1:2, :]

    def exchange(src, dst, send, recv, s, c):
        @pl.loop(1, n_dev)
        def _(i):
            n, where = peer(i)
            remote(src.at[s, c, n], dst.at[s, c, mine], send.at[s, c], recv.at[s, c], where).start()

        pltpu.make_async_copy(src.at[s, c, mine], dst.at[s, c, mine], recv.at[s, c]).start()

    def all_in(dst, recv, s, c):
        pltpu.make_async_copy(dst.at[s, c], dst.at[s, c], recv.at[s, c]).wait()

    def all_out(src, send, s, c):
        part = src.at[s, c, pl.ds(0, n_dev - 1)]
        pltpu.make_async_copy(part, part, send.at[s, c]).wait()

    def pack_send(s, c, match, block):
        picked = jnp.dot(match, block, preferred_element_type=F32)
        pack[s, c] = picked.astype(BF).reshape(n_dev, cap, dc)
        exchange(pack, rx, d_send, d_recv, s, c)

    def one_hot(ref):
        a, b = slot_match(ref)
        return jnp.where(a | b, 1.0, 0.0).astype(BF)

    own = one_hot(info)
    for c in range(chunks):
        pack_send(0, c, own, tok[c])

    @pl.when(jnp.logical_not(inner))
    def _():
        for t in tok_copies:
            t.start()

    info_copy.wait_recv()
    other = one_hot(pinfo)

    def run_experts(s):
        for c in range(chunks):
            all_in(rx, d_recv, s, c)
        ff = wg.shape[1]
        tile = min(256, ff)

        @pl.loop(0, ff // tile)
        def _(f):
            cols = pl.ds(pl.multiple_of(f * tile, tile), tile)
            gate = jnp.zeros((slots, tile), F32)
            up = jnp.zeros((slots, tile), F32)
            for c in range(chunks):
                x = rx[s, c].reshape(slots, dc)
                gate = gate + jnp.dot(x, wg[c * dc : (c + 1) * dc, cols], preferred_element_type=F32)
                up = up + jnp.dot(x, wu[c * dc : (c + 1) * dc, cols], preferred_element_type=F32)
            hid[:, cols] = (gate * jax.nn.sigmoid(gate) * up).astype(BF)

        for c in range(chunks):
            y = jnp.dot(hid[...], wd[:, c * dc : (c + 1) * dc], preferred_element_type=F32)
            ys[s, c] = y.astype(BF).reshape(n_dev, cap, dc)
            if s == 1:
                exchange(ys, yr, r_send, r_recv, s, c)

    tok_copies[0].wait_recv()
    pack_send(1, 0, other, ptok[0])
    for w in weights[1:]:
        w.wait()
    run_experts(0)
    for c in range(1, chunks):
        tok_copies[c].wait_recv()
        pack_send(1, c, other, ptok[c])
    exchange(ys, yr, r_send, r_recv, 0, 0)
    run_experts(1)
    for c in range(1, chunks):
        exchange(ys, yr, r_send, r_recv, 0, c)

    def mix_matrix(ref):
        a, b = slot_match(ref)
        full = jnp.where(a, ref[2:3, :], 0.0) + jnp.where(b, ref[3:4, :], 0.0)
        high = full.astype(BF)
        return high, (full - high.astype(F32)).astype(BF)

    def combine(s, c, mats):
        y = yr[s, c].reshape(slots, dc)
        dims = (((0,), (0,)), ((), ()))
        return sum(lax.dot_general(m, y, dims, preferred_element_type=F32) for m in mats)

    other_mix = mix_matrix(pinfo)
    parts = []
    for c in range(chunks):
        all_in(yr, r_recv, 1, c)
        ps[c] = combine(1, c, other_mix).astype(BF)
        copy = remote(ps.at[c], pr.at[c], pp_sem.at[0, c], pp_sem.at[1, c], partner)
        copy.start()
        parts.append(copy)
    own_mix = mix_matrix(info)
    for c in range(chunks):
        all_in(yr, r_recv, 0, c)
        acc[:, c * dc : (c + 1) * dc] += combine(0, c, own_mix)
    for c in range(chunks):
        parts[c].wait_recv()
        out[:, c * dc : (c + 1) * dc] = (acc[:, c * dc : (c + 1) * dc] + pr[c].astype(F32)).astype(BF)
    info_copy.wait_send()
    gain_copy.wait_send()
    conv_copy.wait_send()

    @pl.when(has_low)
    def _():
        to_low.wait_send()

    @pl.when(has_high)
    def _():
        to_high.wait_send()

    for c in range(chunks):
        tok_copies[c].wait_send()
        parts[c].wait_send()
        for s in range(2):
            all_out(pack, d_send, s, c)
            all_out(ys, r_send, s, c)


def layer_call(resid, value_in, gate_in, taps_w, gain, ffn_gain, routes, ow, w_gate, w_up, w_down, cap):
    sp_count, tp_count = lax.axis_size("sp"), lax.axis_size("tp")
    chunks = 2
    rows, width = resid.shape
    length, local_width = value_in.shape
    halo = (taps_w.shape[0] // 2 + 15) // 16 * 16
    n_dev = sp_count // 2 * tp_count
    dc = width // chunks
    ff = w_gate.shape[1]
    vm = pl.BlockSpec(memory_space=pltpu.VMEM)
    hb = pl.BlockSpec(memory_space=pl.ANY)
    blocks = pltpu.VMEM((2, chunks, n_dev, cap, dc), BF)
    dma = pltpu.SemaphoreType.DMA
    return pl.pallas_call(
        functools.partial(layer_kernel, sp_count, tp_count, cap, chunks),
        out_shape=jax.ShapeDtypeStruct((rows, width), BF),
        in_specs=[vm] * 7 + [hb] * 4,
        out_specs=vm,
        scratch_shapes=[
            pltpu.VMEM((width, ff), BF),
            pltpu.VMEM((width, ff), BF),
            pltpu.VMEM((ff, width), BF),
            pltpu.VMEM((chunks, rows, dc), BF),
            pltpu.VMEM(routes.shape, F32),
            blocks,
            blocks,
            pltpu.VMEM((n_dev * cap, ff), BF),
            blocks,
            blocks,
            pltpu.VMEM((chunks, rows, dc), BF),
            pltpu.VMEM((chunks, rows, dc), BF),
            pltpu.VMEM((rows, width), F32),
            pltpu.VMEM((chunks, rows, dc), BF),
            pltpu.VMEM(routes.shape, F32),
            pltpu.VMEM(ow.shape, BF),
            pltpu.VMEM((length + 2 * halo, local_width), BF),
            pltpu.VMEM((length + 2 * halo, local_width), F32),
            pltpu.VMEM((rows, local_width), F32),
            pltpu.VMEM((2, rows, local_width), F32),
            pltpu.VMEM(gain.shape, F32),
            dma((4,)),
            dma((2,)),
            dma((2, chunks)),
            dma((2, chunks)),
            dma((2, chunks)),
            dma((2, chunks)),
            dma((2, chunks)),
            dma((2, chunks)),
            dma((4,)),
            dma((2,)),
            dma((2,)),
        ],
        compiler_params=pltpu.CompilerParams(
            collective_id=0, has_side_effects=True, vmem_limit_bytes=56 * 1024 * 1024
        ),
        name="layer",
    )(resid, value_in, gate_in, taps_w, gain, ffn_gain, routes, ow, w_gate, w_up, w_down)


def per_device(
    resid,
    value_in,
    gate_in,
    conv_weight,
    norm_gain,
    out_weight,
    ffn_gain,
    expert_ids,
    expert_mix,
    w_gate,
    w_up,
    w_down,
):
    experts_all = lax.axis_size("sp") * lax.axis_size("tp")
    rows_here = resid.shape[0]
    topk = expert_ids.shape[1]
    cap = max(2, (2 * topk * rows_here + experts_all - 1) // experts_all)
    routes = jnp.concatenate(
        [expert_ids.astype(F32), expert_mix, jnp.zeros((rows_here, 8 - 2 * topk), F32)], axis=1
    ).T
    return layer_call(
        resid, value_in, gate_in, conv_weight, norm_gain[None], ffn_gain[None], routes,
        out_weight, w_gate[0], w_up[0], w_down[0], cap,
    )


def solution(mesh):
    return jax.shard_map(
        per_device,
        mesh=mesh,
        in_specs=(
            P(("sp", "tp"), None),
            P("sp", "tp"),
            P("sp", "tp"),
            P(None, "tp"),
            P("tp"),
            P(),
            P(),
            P(("sp", "tp"), None),
            P(("sp", "tp"), None),
            P(("sp", "tp"), None, None),
            P(("sp", "tp"), None, None),
            P(("sp", "tp"), None, None),
        ),
        out_specs=P(("sp", "tp"), None),
        check_vma=False,
    )
```

time: 126 us -> 95.6 us (0.76); the launches traced: 124 us -> 95.3 us
  other arithmetic: 10.3 us -> 2.02 us
  blocking collectives: 6.52 us -> 0 us
  starting transfers between devices: 6.16 us -> 0 us
  matrix products: 4.04 us -> 0 us
  Pallas kernels: 92.4 us -> 90.1 us
  local copies, waits for them, and re-layouts: 4.82 us -> 3.24 us
    ppermute x2 -> x0, starting transfers between devices: 6.16 us -> none  [the longest x1 4.87 us: padded_2(): lax.ppermute(lax.slice_in_dim(block, block.shape[dim] - width, None, axis...]
    reduce_sum x3 -> x0, other arithmetic: 5.56 us -> none  [the longest x1 4.16 us: per_device(): sums = lax.psum((jnp.sum(conv, axis=1), jnp.sum(conv * conv, axis=1)), 'tp')]
    all_to_all x1 -> x0, blocking collectives: 4.05 us -> none  [per_device(): lax.all_to_all(mixed, 'tp', split_axis=0, concat_axis=1, tiled=True)]
    dot_general x2 -> x0, matrix products: 4.04 us -> none  [the longest x1 3.9 us: per_device(): proj = jnp.dot(regrouped, out_weight, preferred_element_type=F32)]
    slice x3 -> x0, local copies, waits for them, and re-layouts: 2.62 us -> none  [the longest x2 2.61 us: per_device(): conv = conv + padded[tap:tap + length] * conv_weight[tap]]
    psum x1 -> x0, blocking collectives: 2.47 us -> none  [per_device(): sums = lax.psum((jnp.sum(conv, axis=1), jnp.sum(conv * conv, axis=1)), 'tp')]
    pallas_call x1, Pallas kernels: 92.4 us -> 90.1 us  [layer_call(): pl.pallas_call(functools.partial(layer_kernel, sp_count, tp_count, cap, c...]
    convert_element_type x4 -> x1, other arithmetic: 2.74 us -> 0.68 us  [per_device(): expert_ids.astype(F32)]
  transfers between devices with their start and end apart: 2 -> 0, of which waited for: 0 -> 0; matrix products, arithmetic and copies ran while one was open for 5% -> 0% of each run, Pallas kernels for 0% -> 0%
where the time goes in v2:
time: 95.6 us; the launch traced here: 95.3 us
  Pallas kernels  90.1 us (94%)
  local copies, waits for them, and re-layouts  3.24 us (3%)
  other arithmetic  2.02 us (2%)
    pallas_call x1, Pallas kernels, layer_call(): pl.pallas_call(functools.partial(layer_kernel, sp_count, tp_count, cap, c...  90.1 us

profile of v2, /device:TPU:0, one launch (start us, length us, event | category | flops | bytes accessed | tf_op | source)
XLA Modules:
  0.0 95.3 jit_solution(12086980336412125227)
XLA Ops:
  0.0 0.1 pad.2.clone
  0.1 0.7 convert_element_type.3
  0.8 1.3 %maximum_bitcast_fusion.routes = f32[8,128]{1,0:T(8,128)} fusion(f32[128,2]{0,1:T(2,128)} %param.20, f32[128,2]{0,1:T(2,128)S(1)} %convert_element_type.3, f32[8]{0:T(128)S(1)} %pad.2.clone), kind=kLoop, calls=%fused_computation | loop fusion | flops 2048 | bytes 6176 | tf_op jit(solution)/shard_map/transpose | solution.py:408
  2.1 1.3 %broadcast_in_dim.9.gain = f32[1,768]{1,0:T(1,128)} reshape(f32[768]{0:T(1024)} %param.16) | data formatting | bytes 6144 | tf_op jit(solution)/shard_map/broadcast_in_dim | solution.py:410
  3.4 90.1 %layer.1 = bf16[128,2048]{1,0:T(8,128)(2,1)} custom-call(bf16[128,2048]{1,0:T(8,128)(2,1)} %resid.1, bf16[256,768]{1,0:T(8,128)(2,1)} %value_in.1, bf16[256,768]{1,0:T(8,128)(2,1)} %gate_in.1, f32[31,768]{1,0:T(8,128)} %taps_w.1, f32[1,768]{1,0:T(1,128)} %broadcast_in_dim.9.gain, f32[1,2048]{1,0:T(1,128)} %bitcast.9, f32[8,128]{1,0:T(8,128)} %maximum_bitcast_fusion.routes, ...), custom_call_target="tpu_custom_call" | custom-call | tf_op jit(solution)/shard_map/layer/pallas_call | solution.py:342
  93.5 1.9 %copy.14 = bf16[128,2048]{1,0:T(8,128)(2,1)} copy(bf16[128,2048]{1,0:T(8,128)(2,1)} %layer.1) | data formatting | bytes 1048576
  (1 shorter events, 0.0 us)

commit v3 on v2

--- a/solution.py
+++ b/solution.py
@@ -13,7 +13,7 @@
 
 def layer_kernel(
     sp_count, tp_count, cap, chunks,
-    resid, value_in, gate_in, taps_w, gain, ffn_gain, routes, ow_h, wg_h, wu_h, wd_h, out,
+    resid, value_in, gate_in, taps_w, gain, ffn_gain, ids, mix, ow_h, wg_h, wu_h, wd_h, out,
     wg, wu, wd, ptok, pinfo, pack, rx, hid, ys, yr, ps, pr, acc,
     tok, info, ow, gp, wide_in, cs, cf, gf,
     w_sem, pi_sem, pt_sem, d_send, d_recv, r_send, r_recv, pp_sem,
@@ -106,14 +106,16 @@
 
     experts_all = sp_count * tp_count
     expert = lax.broadcasted_iota(jnp.int32, (experts_all, rows), 0).astype(F32)
-    hot = [jnp.where(expert == routes[k : k + 1, :], 1.0, 0.0) for k in range(2)]
+    named = ids[...].astype(F32)
+    hot = [jnp.where(expert == named[k : k + 1, :], 1.0, 0.0) for k in range(2)]
     earlier = lax.broadcasted_iota(jnp.int32, (rows, rows), 0)
     later = lax.broadcasted_iota(jnp.int32, (rows, rows), 1)
     before = jnp.where(earlier < later, 1.0, 0.0).astype(BF)
     rank = jnp.dot((hot[0] + hot[1]).astype(BF), before, preferred_element_type=F32)
-    info[...] = routes[...]
+    info[2:4, :] = mix[...]
+    info[4:, :] = jnp.zeros_like(info[4:, :])
     for k in range(2):
-        info[k : k + 1, :] = routes[k : k + 1, :] * cap + jnp.sum(
+        info[k : k + 1, :] = named[k : k + 1, :] * cap + jnp.sum(
             hot[k] * rank, axis=0, keepdims=True
         )
     info_copy = remote(info, pinfo, pi_sem.at[0], pi_sem.at[1], partner)
@@ -170,8 +172,8 @@
         return v * jax.nn.sigmoid(v)
 
     mixed = [
-        silu((cf[0] - mean) * scale * gain[...]).astype(BF),
-        silu((cf[1] - mean) * scale * gf[...]).astype(BF),
+        silu((cf[0] - mean) * scale * gain[...].reshape(1, local_width)).astype(BF),
+        silu((cf[1] - mean) * scale * gf[...].reshape(1, local_width)).astype(BF),
     ]
     whose = (me_tp, 1 - me_tp)
     square = jnp.zeros((rows, 1), F32)
@@ -267,17 +269,20 @@
             if s == 1:
                 exchange(ys, yr, r_send, r_recv, s, c)
 
-    tok_copies[0].wait_recv()
-    pack_send(1, 0, other, ptok[0])
+    early = chunks // 2
+    for c in range(early):
+        tok_copies[c].wait_recv()
+        pack_send(1, c, other, ptok[c])
     for w in weights[1:]:
         w.wait()
     run_experts(0)
-    for c in range(1, chunks):
+    for c in range(early, chunks):
         tok_copies[c].wait_recv()
         pack_send(1, c, other, ptok[c])
-    exchange(ys, yr, r_send, r_recv, 0, 0)
+    for c in range(early):
+        exchange(ys, yr, r_send, r_recv, 0, c)
     run_experts(1)
-    for c in range(1, chunks):
+    for c in range(early, chunks):
         exchange(ys, yr, r_send, r_recv, 0, c)
 
     def mix_matrix(ref):
@@ -326,9 +331,9 @@
             all_out(ys, r_send, s, c)
 
 
-def layer_call(resid, value_in, gate_in, taps_w, gain, ffn_gain, routes, ow, w_gate, w_up, w_down, cap):
+def layer_call(resid, value_in, gate_in, taps_w, gain, ffn_gain, ids, mix, ow, w_gate, w_up, w_down, cap):
     sp_count, tp_count = lax.axis_size("sp"), lax.axis_size("tp")
-    chunks = 2
+    chunks = 4
     rows, width = resid.shape
     length, local_width = value_in.shape
     halo = (taps_w.shape[0] // 2 + 15) // 16 * 16
@@ -342,14 +347,14 @@
     return pl.pallas_call(
         functools.partial(layer_kernel, sp_count, tp_count, cap, chunks),
         out_shape=jax.ShapeDtypeStruct((rows, width), BF),
-        in_specs=[vm] * 7 + [hb] * 4,
+        in_specs=[vm] * 8 + [hb] * 4,
         out_specs=vm,
         scratch_shapes=[
             pltpu.VMEM((width, ff), BF),
             pltpu.VMEM((width, ff), BF),
             pltpu.VMEM((ff, width), BF),
             pltpu.VMEM((chunks, rows, dc), BF),
-            pltpu.VMEM(routes.shape, F32),
+            pltpu.VMEM((8, rows), F32),
             blocks,
             blocks,
             pltpu.VMEM((n_dev * cap, ff), BF),
@@ -359,7 +364,7 @@
             pltpu.VMEM((chunks, rows, dc), BF),
             pltpu.VMEM((rows, width), F32),
             pltpu.VMEM((chunks, rows, dc), BF),
-            pltpu.VMEM(routes.shape, F32),
+            pltpu.VMEM((8, rows), F32),
             pltpu.VMEM(ow.shape, BF),
             pltpu.VMEM((length + 2 * halo, local_width), BF),
             pltpu.VMEM((length + 2 * halo, local_width), F32),
@@ -379,10 +384,10 @@
             dma((2,)),
         ],
         compiler_params=pltpu.CompilerParams(
-            collective_id=0, has_side_effects=True, vmem_limit_bytes=56 * 1024 * 1024
+            collective_id=0, has_side_effects=True, vmem_limit_bytes=58 * 1024 * 1024
         ),
         name="layer",
-    )(resid, value_in, gate_in, taps_w, gain, ffn_gain, routes, ow, w_gate, w_up, w_down)
+    )(resid, value_in, gate_in, taps_w, gain, ffn_gain, ids, mix, ow, w_gate, w_up, w_down)
 
 
 def per_device(
@@ -403,11 +408,8 @@
     rows_here = resid.shape[0]
     topk = expert_ids.shape[1]
     cap = max(2, (2 * topk * rows_here + experts_all - 1) // experts_all)
-    routes = jnp.concatenate(
-        [expert_ids.astype(F32), expert_mix, jnp.zeros((rows_here, 8 - 2 * topk), F32)], axis=1
-    ).T
     return layer_call(
-        resid, value_in, gate_in, conv_weight, norm_gain[None], ffn_gain[None], routes,
+        resid, value_in, gate_in, conv_weight, norm_gain, ffn_gain[None], expert_ids.T, expert_mix.T,
         out_weight, w_gate[0], w_up[0], w_down[0], cap,
     )
 

time: 95.6 us -> 88.6 us (0.927)
  Pallas kernels: 90.1 us -> 86.5 us
  other arithmetic: 2.02 us -> 0 us
  local copies, waits for them, and re-layouts: 3.24 us -> 1.88 us
    pallas_call x1, Pallas kernels: 90.1 us -> 86.5 us  [layer_call(): pl.pallas_call(functools.partial(layer_kernel, sp_count, tp_count, cap, c...]
    transpose x1 -> x0, other arithmetic: 1.34 us -> none  [per_device(): routes = jnp.concatenate([expert_ids.astype(F32), expert_mix, jnp.zeros((...]
    broadcast_in_dim x2 -> x0, local copies, waits for them, and re-layouts: 1.28 us -> none  [the longest x1 1.28 us: per_device(): norm_gain[None]]
where the time goes in v3:
time: 88.6 us; the launch traced here: 88.4 us
  Pallas kernels  86.5 us (98%)
  local copies, waits for them, and re-layouts  1.88 us (2%)
    pallas_call x1, Pallas kernels, layer_call(): pl.pallas_call(functools.partial(layer_kernel, sp_count, tp_count, cap, c...  86.5 us
    unnamed x1, local copies, waits for them, and re-layouts  1.88 us

profile of v3, /device:TPU:0, one launch (start us, length us, event | category | flops | bytes accessed | tf_op | source)
XLA Modules:
  0.0 88.4 jit_solution(10485840765606040127)
XLA Ops:
  0.0 86.5 %layer.1 = bf16[128,2048]{1,0:T(8,128)(2,1)} custom-call(bf16[128,2048]{1,0:T(8,128)(2,1)} %resid.1, bf16[256,768]{1,0:T(8,128)(2,1)} %value_in.1, bf16[256,768]{1,0:T(8,128)(2,1)} %gate_in.1, f32[31,768]{1,0:T(8,128)} %taps_w.1, f32[768]{0:T(1024)} %gain.1, f32[1,2048]{1,0:T(1,128)} %bitcast.9, s32[2,128]{1,0:T(2,128)} %bitcast.10, f32[2,128]{1,0:T(2,128)} %bitcast.11, ...), custom_call_target="tpu_custom_call" | custom-call | tf_op jit(solution)/shard_map/layer/pallas_call | solution.py:347
  86.5 1.9 %copy.14 = bf16[128,2048]{1,0:T(8,128)(2,1)} copy(bf16[128,2048]{1,0:T(8,128)(2,1)} %layer.1) | data formatting | bytes 1048576
